TPU v7x, 32 devices: a whole 2x2x4 slice. The times are simulated.
32 devices in a mesh: sp: 4 (over y, core), tp: 8 (over z, x).
Axes of the slice: x: 2, y: 2, z: 4, core: 2. Of those that a mesh axis runs over, the one named last changes fastest.
Arguments:
- latent: bfloat16 [960, 2048], P(('sp', 'tp')), may hold values from -40 to 40
- context: bfloat16 [768, 2048], P('sp'), may hold values from -6 to 6
- cond_latent: float32 [2048], P('sp'), may hold values from -6 to 6
- cond_context: float32 [2048], P('sp'), may hold values from -6 to 6
- mod_weight: bfloat16 [2048, 6144], P('sp', 'tp'), may hold values from -0.125 to 0.125
- w_query: bfloat16 [2048, 1024], P(None, 'tp'), may hold values from -5 to 5
- w_key: bfloat16 [2048, 1024], P(None, 'tp'), may hold values from -5 to 5
- w_value: bfloat16 [2048, 1024], P(None, 'tp'), may hold values from -0.125 to 0.125
- w_out: bfloat16 [1024, 2048], P('tp'), may hold values from -0.1875 to 0.1875
- head_lambda: float32 [8], P('tp'), may hold values from 0.3 to 0.8
Outputs:
- mixed_latent: bfloat16 [960, 2048], P(('sp', 'tp'))
All inputs are finite; a program needn't handle non-finite values.
Results may differ from a plain program's by a relative error of at most 0.011.
Values may be sent and summed in bfloat16 or wider, within the bound.
A program may use at most 64 MiB of HBM per device.

v0:
```python
import jax
import jax.numpy as jnp
from jax import lax
from jax.sharding import PartitionSpec as P

QK_DIM = 64
VAL_DIM = 128
GRID_W = 64


NORM_EPS = 0.01
HEAD_EPS = 0.001
THETA = 10000.0


def modulate_rows(rows, shift, scale):
    values = rows.astype(jnp.float32)
    normed = values * lax.rsqrt(jnp.mean(values * values, axis=-1, keepdims=True) + NORM_EPS)
    return (normed * (1.0 + scale) + shift).astype(jnp.bfloat16)


def rotary_tables(positions):
    quarter = QK_DIM // 4
    inverse = THETA ** (-jnp.arange(quarter, dtype=jnp.float32) / quarter)
    grid_row = (positions // GRID_W).astype(jnp.float32)
    grid_column = (positions % GRID_W).astype(jnp.float32)
    by_row = grid_row[:, None] * inverse[None, :]
    by_column = grid_column[:, None] * inverse[None, :]
    angle = jnp.concatenate([by_row, by_row, by_column, by_column], axis=-1)
    return (jnp.cos(angle), jnp.sin(angle))


def rotate(product, cosine, sine):
    number = product.shape[0]
    quarter = QK_DIM // 4
    half = QK_DIM // 2
    shaped = product.reshape(number, -1, QK_DIM)
    first = shaped[..., :half]
    second = shaped[..., half:]
    turned = jnp.concatenate(
        [
            -first[..., quarter:],
            first[..., :quarter],
            -second[..., quarter:],
            second[..., :quarter],
        ],
        axis=-1,
    )
    result = shaped * cosine[:, None, :] + turned * sine[:, None, :]
    return result.reshape(number, -1).astype(jnp.bfloat16)


def attend_piece(state, piece, queries):
    highest, totals, carried = state
    keys, values = piece
    number = keys.shape[0]
    heads = queries.shape[1]
    key_heads = keys.reshape(number, heads, 2, QK_DIM)
    value_heads = values.reshape(number, heads, VAL_DIM)
    scores = jnp.einsum(
        "qhmd,khmd->hmqk", queries, key_heads, preferred_element_type=jnp.float32
    ) * QK_DIM ** (-0.5)
    new_highest = jnp.maximum(highest, jnp.max(scores, axis=-1))
    weights = jnp.exp(scores - new_highest[..., None])
    totals = jnp.sum(weights, axis=-1)
    mixed = jnp.einsum(
        "hmqk,khd->hmqd",
        weights.astype(jnp.bfloat16),
        value_heads,
        preferred_element_type=jnp.float32,
    )
    carried = mixed
    return (new_highest, totals, carried)


def shards(
    latent,
    context,
    cond_latent,
    cond_context,
    mod_weight,
    w_query,
    w_key,
    w_value,
    w_out,
    head_lambda,
):
    width = latent.shape[1]
    heads = head_lambda.shape[0]
    conditioned = jax.nn.silu(jnp.stack([cond_latent, cond_context])).astype(jnp.bfloat16)
    partial_mod = jnp.dot(conditioned, mod_weight, preferred_element_type=jnp.float32)
    summed = lax.psum(partial_mod, "sp")
    modulation = lax.all_gather(summed, "tp", axis=1, tiled=True)
    shift_context = modulation[1, :width]
    scale_context = modulation[1, width : 2 * width]
    gate_latent = modulation[0, 2 * width :]
    own_rows = modulate_rows(latent, modulation[0, :width], modulation[0, width : 2 * width])
    group_rows = latent.shape[0] * lax.axis_size("tp")
    offset = lax.axis_index("sp") * group_rows
    piece = lax.all_gather(own_rows, "tp", axis=0, tiled=True)
    positions = offset + jnp.arange(piece.shape[0], dtype=jnp.int32)
    cosine, sine = rotary_tables(positions)
    query_part = rotate(jnp.dot(piece, w_query, preferred_element_type=jnp.float32), cosine, sine)
    key_part = rotate(jnp.dot(piece, w_key, preferred_element_type=jnp.float32), cosine, sine)
    value_part = jnp.dot(piece, w_value, preferred_element_type=jnp.float32).astype(jnp.bfloat16)
    projected = jnp.concatenate([query_part, key_part, value_part], axis=1)
    key_columns = heads * 2 * QK_DIM
    queries = projected[:, :key_columns].reshape(group_rows, heads, 2, QK_DIM)
    keys = projected[:, key_columns : 2 * key_columns]
    values = projected[:, 2 * key_columns :]
    initial = (
        jnp.full((heads, 2, group_rows), -1e30, jnp.float32),
        jnp.zeros((heads, 2, group_rows), jnp.float32),
        jnp.zeros((heads, 2, group_rows, VAL_DIM), jnp.float32),
    )
    own_context = modulate_rows(context, shift_context, scale_context)
    context_keys = jnp.dot(own_context, w_key, preferred_element_type=jnp.float32).astype(
        jnp.bfloat16
    )
    context_values = jnp.dot(own_context, w_value, preferred_element_type=jnp.float32).astype(
        jnp.bfloat16
    )
    joined_keys = jnp.concatenate([keys, context_keys], axis=0)
    joined_values = jnp.concatenate([values, context_values], axis=0)
    state = attend_piece(
        initial,
        (
            lax.all_gather(joined_keys, "sp", axis=0, tiled=True),
            lax.all_gather(joined_values, "sp", axis=0, tiled=True),
        ),
        queries,
    )
    highest, totals, carried = state
    factor = head_lambda[:, None, None]
    head_out = (
        carried[:, 0] / totals[:, 0][..., None] - factor * carried[:, 1] / totals[:, 1][..., None]
    )
    head_out = head_out * lax.rsqrt(
        jnp.mean(head_out * head_out, axis=-1, keepdims=True) + HEAD_EPS
    )
    attended = (
        jnp.transpose(head_out, (1, 0, 2)).reshape(group_rows, heads * VAL_DIM).astype(jnp.bfloat16)
    )
    branch = lax.psum_scatter(
        jnp.dot(attended, w_out, preferred_element_type=jnp.float32),
        "tp",
        scatter_dimension=0,
        tiled=True,
    )
    branch = branch * lax.rsqrt(jnp.mean(branch * branch, axis=-1, keepdims=True) + NORM_EPS)
    return (latent.astype(jnp.float32) + gate_latent * branch).astype(jnp.bfloat16)


def solution(mesh):
    placed = (
        P(("sp", "tp"), None),
        P("sp", None),
        P("sp"),
        P("sp"),
        P("sp", "tp"),
        P(None, "tp"),
        P(None, "tp"),
        P(None, "tp"),
        P("tp", None),
        P("tp"),
    )
    return jax.shard_map(
        shards, mesh=mesh, in_specs=placed, out_specs=P(("sp", "tp"), None), check_vma=False
    )
```

profile of v0, /device:TPU:0, one launch (start us, length us, event | category | flops | bytes accessed | tf_op | source)
XLA Modules:
  0.0 153.2 jit_solution(12564381263375404381)
XLA Ops:
  0.0 0.0 copy-start
  0.0 1.1 fusion.14
  1.1 0.0 copy-start.2
  1.2 0.0 copy-start.3
  1.2 1.5 fusion.6
  2.6 0.0 copy-done
  2.7 0.9 fusion.37
  3.6 8.5 %psum.7 = f32[2,768]{1,0:T(2,128)S(1)} all-reduce(f32[2,768]{1,0:T(2,128)S(1)} %fusion.37), channel_id=1, replica_groups=mesh['sp'=4,'tp'=8] {'sp'}, use_global_device_ids=true, to_apply=%region_0.1 | all-reduce | flops 1536 | bytes 12288 | tf_op jit(solution)/shard_map/psum | solution.py:92
  12.1 31.1 %all_gather.12 = f32[2,6144]{1,0:T(2,128)S(1)} all-gather(f32[2,768]{1,0:T(2,128)S(1)} %psum.7), channel_id=1, replica_groups=mesh['sp'=4,'tp'=8] {'tp'}, dimensions={1}, use_global_device_ids=true | all-gather | bytes 55296 | tf_op jit(solution)/shard_map/all_gather | solution.py:93
  43.3 0.0 copy-start.1
  43.3 1.8 %convolution_convert_fusion.1 = bf16[192,128]{1,0:T(8,128)(2,1)S(1)} fusion(bf16[2048,128]{1,0:T(8,128)(2,1)} %param.17, bf16[192,2048]{1,0:T(8,128)(2,1)} %param.11, f32[2048]{0:T(1024)S(1)} %bitcast.84, f32[2048]{0:T(1024)S(1)} %bitcast.86, f32[192]{0:T(256)S(1)} %add_rsqrt_fusion.1), kind=kOutput, calls=%fused_computation.14 | convolution fusion | flops 102653952 | bytes 1377024 | tf_op jit(solution)/shard_map/dot_general | solution.py:120
  45.0 0.0 copy-done.2
  45.1 0.0 copy-done.3
  45.1 0.5 convolution_convert_fusion.2
  45.5 0.0 copy-done.1
  45.5 0.1 fusion.19
  45.7 32.9 %all-gather = bf16[8,30,2048]{2,1,0:T(8,128)(2,1)S(1)} all-gather(bf16[1,30,2048]{2,1,0:T(8,128)(2,1)S(1)} %fusion.19), channel_id=1, replica_groups=mesh['sp'=4,'tp'=8] {'tp'}, dimensions={0}, use_global_device_ids=true | all-gather | bytes 1105920 | tf_op jit(solution)/shard_map/all_gather | solution.py:100
  78.6 0.3 reshape.355
  78.8 0.0 copy-start.4
  78.9 1.5 convolution_convert_fusion
  80.4 1.4 fusion.49
  82.5 0.1 broadcast_multiply_fusion.1
  82.6 0.1 fusion.35
  82.7 0.1 copy.21
  82.8 0.0 copy-done.4
  82.8 0.4 fusion.48
  83.2 0.1 copy.22
  83.3 0.1 copy.26
  83.5 0.1 copy.27
  83.6 0.1 copy.23
  83.7 0.1 copy.24
  83.9 6.3 %all_gather.14 = bf16[1728,128]{1,0:T(8,128)(2,1)S(1)} all-gather(bf16[432,128]{1,0:T(8,128)(2,1)S(1)} %pad_maximum_fusion), channel_id=1, replica_groups=mesh['sp'=4,'tp'=8] {'sp'}, dimensions={0}, use_global_device_ids=true | all-gather | bytes 552960 | tf_op jit(solution)/shard_map/all_gather | solution.py:128
  90.2 0.2 copy.28
  90.4 6.8 %all_gather.15 = bf16[1728,128]{1,0:T(8,128)(2,1)S(1)} all-gather(bf16[432,128]{1,0:T(8,128)(2,1)S(1)} %pad_maximum_fusion.1), channel_id=1, replica_groups=mesh['sp'=4,'tp'=8] {'sp'}, dimensions={0}, use_global_device_ids=true | all-gather | bytes 552960 | tf_op jit(solution)/shard_map/all_gather | solution.py:129
  97.2 0.7 fusion.47
  98.0 0.6 fusion.1
  98.6 0.0 copy-start.5
  98.6 0.7 fusion.10
  99.3 0.2 fusion.27
  99.5 0.1 copy-done.5
  99.6 0.0 copy-start.6
  99.6 0.5 fusion.28
  100.1 46.5 %fusion = f32[32,2048]{1,0:T(8,128)S(1)} fusion(f32[240,2048]{1,0:T(8,128)S(1)} %fusion.28), kind=kCustom, calls=%all-reduce-scatter | all-reduce-scatter fusion | flops 524289 | bytes 2228736
  146.6 2.9 %collective-permute-start = (f32[14,2048]{1,0:T(8,128)S(1)}, f32[14,2048]{1,0:T(8,128)S(1)}, u32[]{:S(2)}, u32[]{:S(2)}) collective-permute-start(f32[14,2048]{1,0:T(8,128)S(1)} %slice.97), channel_id=1, source_target_pairs={{0,1},{1,2},{2,3},{3,4},{4,5},{5,6},{6,7},{8,9},{9,10},{10,11},{11... | collective-permute-start | bytes 344072
  149.5 0.0 copy-done.6
  149.6 0.6 dynamic-slice.4
  150.8 1.2 collective-permute-done
  152.0 0.2 concatenate.28
  152.3 0.2 multiply_reduce_fusion
  152.5 0.8 fusion.18
  (16 shorter events, 0.2 us)
Async XLA Ops:
  0.0 2.6 %copy-start = (bf16[512,768]{1,0:T(8,128)(2,1)S(1)}, bf16[512,768]{1,0:T(8,128)(2,1)}, u32[]{:S(2)}) copy-start(bf16[512,768]{1,0:T(8,128)(2,1)} %param.14) | copy-start | bytes 2359300
  1.1 43.9 %copy-start.2 = (bf16[192,2048]{1,0:T(8,128)(2,1)S(1)}, bf16[192,2048]{1,0:T(8,128)(2,1)}, u32[]{:S(2)}) copy-start(bf16[192,2048]{1,0:T(8,128)(2,1)} %param.11) | copy-start | bytes 2359300
  1.2 43.9 %copy-start.3 = (bf16[2048,128]{1,0:T(8,128)(2,1)S(1)}, bf16[2048,128]{1,0:T(8,128)(2,1)}, u32[]{:S(2)}) copy-start(bf16[2048,128]{1,0:T(8,128)(2,1)} %param.16) | copy-start | bytes 1572868
  43.3 2.3 %copy-start.1 = (bf16[30,2048]{1,0:T(8,128)(2,1)S(1)}, bf16[30,2048]{1,0:T(8,128)(2,1)}, u32[]{:S(2)}) copy-start(bf16[30,2048]{1,0:T(8,128)(2,1)} %param.10) | copy-start | bytes 368644
  78.8 4.0 %copy-start.4 = (bf16[2048,128]{1,0:T(8,128)(2,1)S(1)}, bf16[2048,128]{1,0:T(8,128)(2,1)}, u32[]{:S(2)}) copy-start(bf16[2048,128]{1,0:T(8,128)(2,1)} %param.15) | copy-start | bytes 1572868
  98.6 1.0 copy-start.5
  99.6 49.9 %copy-start.6 = (u32[32]{0:T(128)S(1)}, u32[32]{0:T(128)}, u32[]{:S(2)}) copy-start(u32[32]{0:T(128)} %constant.70) | copy-start | bytes 388
  146.6 5.4 %collective-permute-start = (f32[14,2048]{1,0:T(8,128)S(1)}, f32[14,2048]{1,0:T(8,128)S(1)}, u32[]{:S(2)}, u32[]{:S(2)}) collective-permute-start(f32[14,2048]{1,0:T(8,128)S(1)} %slice.97), channel_id=1, source_target_pairs={{0,1},{1,2},{2,3},{3,4},{4,5},{5,6},{6,7},{8,9},{9,10},{10,11},{11... | collective-permute-start | bytes 344072
where the time goes:
time: 154 us; the launch traced here: 153 us
  blocking collectives  132 us (86%)
  matrix products  8.4 us (5%)
  other arithmetic  4.88 us (3%)
  starting transfers between devices  2.92 us (2%)
  local copies, waits for them, and re-layouts  2.05 us (1%)
  between operations  1.61 us (1%)
    unnamed x1, blocking collectives  46.5 us
    all_gather x1, blocking collectives, shards(): piece = lax.all_gather(own_rows, 'tp', axis=0, tiled=True)  32.9 us
    all_gather x1, blocking collectives, shards(): modulation = lax.all_gather(summed, 'tp', axis=1, tiled=True)  31.1 us
    psum x1, blocking collectives, shards(): summed = lax.psum(partial_mod, 'sp')  8.52 us
    all_gather x1, blocking collectives, shards(): lax.all_gather(joined_values, 'sp', axis=0, tiled=True)  6.83 us
    all_gather x1, blocking collectives, shards(): lax.all_gather(joined_keys, 'sp', axis=0, tiled=True)  6.28 us
  transfers between devices with their start and end apart: 1, of which 1 were waited for; matrix products, arithmetic and copies ran while one was open for 0% of the time, Pallas kernels for 0%

commit v1 on v0

v1 whole, which is shorter than its diff:
```python
import functools

import jax
import jax.numpy as jnp
import numpy as np
from jax import lax
from jax.experimental import pallas as pl
from jax.experimental.pallas import tpu as pltpu
from jax.sharding import PartitionSpec as P

QK_DIM = 64
VAL_DIM = 128
GRID_W = 64
NORM_EPS = 0.01
HEAD_EPS = 0.001
THETA = 10000.0
F32 = jnp.float32
BF16 = jnp.bfloat16


def rotary_tables(nsp, ntp, rows, padded):
    quarter = QK_DIM // 4
    inverse = np.float32(THETA) ** (-np.arange(quarter, dtype=np.float32) / quarter)
    p = np.arange(nsp * ntp * rows)
    r = (p // GRID_W).astype(np.float32)[:, None] * inverse
    c = (p % GRID_W).astype(np.float32)[:, None] * inverse
    angle = np.concatenate([r, r, c, c] * 2, axis=-1).astype(np.float32)
    sign = np.where(np.arange(2 * QK_DIM) % (2 * quarter) < quarter, -1.0, 1.0)
    both = np.concatenate([np.cos(angle), np.sin(angle) * sign], axis=-1).astype(np.float32)
    full = np.zeros((nsp * ntp, padded, 4 * QK_DIM), np.float32)
    full[:, :rows] = both.reshape(nsp * ntp, rows, -1)
    return full.reshape(nsp, ntp * padded, -1)


def kernel(
    nsp, ntp, rows, padded, ctx, width, modcols, qb,
    latent, context, condl, condc, modw, wq, wk, wv, wout, lam, table,
    out,
    raw, ctxv, modwv, wcat, wo, tab, part, mods, nbuf, nctx, kv, qbuf, att, att2, send, outb,
    loc, rsend, rrecv, p1s, p1r, p2s, p2r, kvs, kvf, kvr, ws, wr, ats, atr, os, orr,
):
    sp, tp = lax.axis_index("sp"), lax.axis_index("tp")
    zn, yn = ntp // 2, nsp // 2
    zi, xi = tp // 2, lax.rem(tp, 2)
    yi, ci = sp // 2, lax.rem(sp, 2)
    xpeer = zi * 2 + (1 - xi)
    cpeer = yi * 2 + (1 - ci)
    latrows = ntp * padded
    block_rows = latrows + ctx

    def local(i, src, dst):
        return pltpu.make_async_copy(src, dst, loc.at[i])

    def remote(src, dst, ss, rs, to_sp, to_tp):
        return pltpu.make_async_remote_copy(
            src_ref=src, dst_ref=dst, send_sem=ss, recv_sem=rs,
            device_id=(to_sp, to_tp), device_id_type=pl.DeviceIdType.MESH,
        )

    copies = [
        local(0, latent, raw.at[tp]),
        local(1, modw, modwv),
        local(2, context, ctxv),
        local(3, wk, wcat.at[:, pl.ds(0, 128)]),
        local(4, wv, wcat.at[:, pl.ds(128, 128)]),
        local(5, wq, wcat.at[:, pl.ds(256, 128)]),
        local(6, table.at[sp], tab),
        local(7, wout, wo.at[xi]),
    ]
    for c in copies:
        c.start()

    barrier = pltpu.get_barrier_semaphore()

    @pl.loop(1, ntp)
    def _(d):
        pl.semaphore_signal(
            barrier, inc=1, device_id=(sp, lax.rem(tp + d, ntp)),
            device_id_type=pl.DeviceIdType.MESH,
        )

    @pl.loop(1, nsp)
    def _(d):
        pl.semaphore_signal(
            barrier, inc=1, device_id=(lax.rem(sp + d, nsp), tp),
            device_id_type=pl.DeviceIdType.MESH,
        )

    copies[1].wait()
    cl = jax.nn.silu(condl[...]).reshape(1, -1)
    cc = jax.nn.silu(condc[...]).reshape(1, -1)
    row = lax.broadcasted_iota(jnp.int32, (8, cl.shape[1]), 0)
    cond = jnp.where(row == 0, cl, jnp.where(row == 1, cc, 0.0)).astype(BF16)
    part[sp] = jnp.dot(cond, modwv[...], preferred_element_type=F32)
    copies[0].wait()
    pl.semaphore_wait(barrier, (ntp - 1) + (nsp - 1))

    def p1(d, src):
        return remote(part.at[src], part.at[src], p1s.at[d], p1r.at[src], lax.rem(sp + d, nsp), tp)

    @pl.loop(1, nsp)
    def _(d):
        p1(d, sp).start()

    def row_copy(way, t, to):
        return remote(raw.at[t], raw.at[t], rsend.at[way, t], rrecv.at[t], sp, to)

    def up(t):
        return row_copy(0, t, lax.rem(tp + 2, ntp))

    def down(t):
        return row_copy(1, t, lax.rem(tp + ntp - 2, ntp))

    def across(t):
        return row_copy(2, t, xpeer)

    def forward(t, from_below):
        if from_below is not False:

            @pl.when(zi < zn - 1)
            def _():
                up(t).start()

        if from_below is not True:

            @pl.when(zi > 0)
            def _():
                down(t).start()

        across(t).start()

    forward(tp, None)
    copies[7].wait()

    def row_step(s):
        @pl.when(zi - s >= 0)
        def _():
            t = tp - 2 * s
            across(t).wait_recv()
            forward(t, True)

        @pl.when(zi + s < zn)
        def _():
            t = tp + 2 * s
            across(t).wait_recv()
            forward(t, False)

    @pl.loop(1, nsp)
    def _(d):
        p1(d, lax.rem(sp + nsp - d, nsp)).wait_recv()

    total = part[0]
    for k in range(1, nsp):
        total = total + part[k]
    mods[tp] = total

    def p2(d, src):
        return remote(mods.at[src], mods.at[src], p2s.at[d], p2r.at[src], sp, lax.rem(tp + d, ntp))

    @pl.loop(1, ntp)
    def _(d):
        p2(d, tp).start()

    row_step(1)

    @pl.loop(1, ntp)
    def _(d):
        p2(d, lax.rem(tp + ntp - d, ntp)).wait_recv()

    mod = jnp.concatenate([mods[t] for t in range(ntp)], axis=1)
    shift_l, shift_c = mod[0:1, :width], mod[1:2, :width]
    scale_l, scale_c = 1.0 + mod[0:1, width : 2 * width], 1.0 + mod[1:2, width : 2 * width]
    gate = mod[0:1, 2 * width :]

    def normed(x, scale, shift):
        x = x.astype(F32)
        x = x * lax.rsqrt(jnp.mean(x * x, axis=-1, keepdims=True) + NORM_EPS)
        return (x * scale + shift).astype(BF16)

    copies[2].wait()
    nctx[...] = normed(ctxv[...], scale_c, shift_c)
    copies[3].wait()
    copies[4].wait()
    lat_part, ctx_part = pl.ds(0, latrows), pl.ds(latrows, ctx)
    kv[sp, latrows:block_rows, :] = jnp.dot(
        nctx[...], wcat[:, 0:256], preferred_element_type=F32
    ).astype(BF16)

    def kv_direct(which, d, src):
        piece = (lat_part, ctx_part)[which]
        return remote(
            kv.at[src, piece], kv.at[src, piece], kvs.at[which, d], kvr.at[which, src],
            lax.rem(sp + 2 * d, nsp), tp,
        )

    def kv_forward(which, src):
        piece = (lat_part, ctx_part)[which]
        return remote(
            kv.at[src, piece], kv.at[src, piece], kvf.at[which, src], kvr.at[which, src], cpeer, tp
        )

    def kv_send(which):
        for d in range(1, yn):
            kv_direct(which, d, sp).start()
        kv_forward(which, sp).start()

    def kv_relay(which):
        for d in range(1, yn):
            src = lax.rem(sp + nsp - 2 * d, nsp)
            kv_direct(which, d, src).wait_recv()
            kv_forward(which, src).start()

    def kv_finish(which):
        for y in range(yn):
            kv_forward(which, y * 2 + (1 - ci)).wait_recv()

    kv_send(1)
    for s in range(2, zn):
        row_step(s)
    wo_copy = remote(wo.at[xi], wo.at[xi], ws, wr.at[xi], sp, xpeer)
    wo_copy.start()
    kv_relay(1)

    nbuf[...] = jnp.zeros_like(nbuf)

    def norm_row(t):
        nbuf[t, 0:rows, :] = normed(raw[t], scale_l, shift_l)

    for z in range(zn):
        norm_row(z * 2 + xi)
    for z in range(zn):
        t = z * 2 + (1 - xi)
        across(t).wait_recv()
        norm_row(t)
    copies[5].wait()
    copies[6].wait()
    x = nbuf[...].reshape(latrows, width)
    pkv = jnp.dot(x, wcat[:, 0:256], preferred_element_type=F32)
    cosine, sine = tab[:, 0:128], tab[:, 128:256]
    quarter = QK_DIM // 4
    lane = lax.broadcasted_iota(jnp.int32, (1, 128), 1)
    low = lax.rem(lane, 2 * quarter) < quarter

    def rotate(u):
        turned = jnp.where(low, pltpu.roll(u, 128 - quarter, 1), pltpu.roll(u, quarter, 1))
        return (u * cosine + turned * sine).astype(BF16)

    kv[sp, 0:latrows, 0:128] = rotate(pkv[:, 0:128])
    kv[sp, 0:latrows, 128:256] = pkv[:, 128:256].astype(BF16)
    kv_send(0)
    q = rotate(jnp.dot(x, wcat[:, 256:384], preferred_element_type=F32)) * BF16(QK_DIM**-0.5)
    qbuf[0] = jnp.where(lane < QK_DIM, q, BF16(0))
    qbuf[1] = jnp.where(lane < QK_DIM, BF16(0), q)
    kv_relay(0)
    kv_finish(1)
    kv_finish(0)

    keys = nsp * block_rows
    col = lax.rem(lax.broadcasted_iota(jnp.int32, (1, keys), 1), block_rows)
    empty = jnp.logical_and(col < latrows, lax.rem(col, padded) >= rows)
    bias = jnp.where(empty, F32(-1e30), F32(0.0))
    factor = lam[0]

    @pl.loop(0, latrows // qb)
    def _(i):
        here = pl.ds(pl.multiple_of(i * qb, qb), qb)
        mixed = []
        for m in range(2):
            s = lax.dot_general(
                qbuf[m, here, :], kv[:, :, 0:128].reshape(keys, 128), (((1,), (1,)), ((), ())),
                preferred_element_type=F32,
            ) + bias
            w = jnp.exp(s - jnp.max(s, axis=-1, keepdims=True))
            t = jnp.sum(w, axis=-1, keepdims=True)
            o = jnp.dot(
                w.astype(BF16), kv[:, :, 128:256].reshape(keys, 128), preferred_element_type=F32
            )
            mixed.append(o / t)
        h = mixed[0] - factor * mixed[1]
        h = h * lax.rsqrt(jnp.mean(h * h, axis=-1, keepdims=True) + HEAD_EPS)
        att[here, :] = h.astype(BF16)

    for z in range(zn):
        for x01 in range(2):
            att2[x01, z] = att[(z * 2 + x01) * padded : (z * 2 + x01 + 1) * padded, :]
    at_copy = remote(att2.at[1 - xi], att2.at[2], ats, atr, sp, xpeer)
    at_copy.start()
    remote(wo.at[1 - xi], wo.at[1 - xi], ws, wr.at[1 - xi], sp, xpeer).wait_recv()
    at_copy.wait_recv()
    w_mine, w_other = wo[xi], wo[1 - xi]

    def out_copy(d, src):
        to = lax.rem(zi + d, zn) * 2 + xi
        return remote(send.at[d], outb.at[src], os.at[d], orr.at[src], sp, to)

    for d in range(zn - 1, -1, -1):
        z = lax.rem(zi + d, zn)
        y = jnp.dot(att2[xi, z], w_mine, preferred_element_type=F32) + jnp.dot(
            att2[2, z], w_other, preferred_element_type=F32
        )
        if d:
            send[d] = y.astype(BF16)
            out_copy(d, zi).start()
    branch = y
    for d in range(1, zn):
        src = lax.rem(zi + zn - d, zn)
        out_copy(d, src).wait_recv()
        branch = branch + outb[src].astype(F32)
    branch = branch * lax.rsqrt(jnp.mean(branch * branch, axis=-1, keepdims=True) + NORM_EPS)
    out[...] = (raw[tp].astype(F32) + gate * branch[:rows]).astype(BF16)

    @pl.loop(1, nsp)
    def _(d):
        p1(d, sp).wait_send()

    @pl.loop(1, ntp)
    def _(d):
        p2(d, tp).wait_send()

    for z in range(zn):
        t = z * 2 + xi

        @pl.when(jnp.logical_and(z <= zi, zi < zn - 1))
        def _():
            up(t).wait_send()

        @pl.when(jnp.logical_and(z >= zi, zi > 0))
        def _():
            down(t).wait_send()

        across(t).wait_send()
    for which in range(2):
        for d in range(1, yn):
            kv_direct(which, d, sp).wait_send()
        for y in range(yn):
            kv_forward(which, y * 2 + ci).wait_send()
    wo_copy.wait_send()
    at_copy.wait_send()
    for d in range(1, zn):
        out_copy(d, zi).wait_send()


def shards(nsp, ntp, latent, context, condl, condc, modw, wq, wk, wv, wout, lam):
    rows, width = latent.shape
    ctx = context.shape[0]
    padded = -(-rows // 16) * 16
    latrows = ntp * padded
    block_rows = latrows + ctx
    modcols = modw.shape[1]
    zn = ntp // 2
    qb = latrows
    while qb % 32 == 0 and qb * nsp * block_rows * 4 > 1_000_000:
        qb //= 2
    table = jnp.asarray(rotary_tables(nsp, ntp, rows, padded))
    anyspace = pl.BlockSpec(memory_space=pl.ANY)
    vmem = pl.BlockSpec(memory_space=pltpu.VMEM)
    smem = pl.BlockSpec(memory_space=pltpu.SMEM)
    dma = pltpu.SemaphoreType.DMA
    return pl.pallas_call(
        functools.partial(kernel, nsp, ntp, rows, padded, ctx, width, modcols, qb),
        out_shape=jax.ShapeDtypeStruct((rows, width), BF16),
        in_specs=[anyspace, anyspace, vmem, vmem] + [anyspace] * 5 + [smem, anyspace],
        out_specs=vmem,
        scratch_shapes=[
            pltpu.VMEM((ntp, rows, width), BF16),
            pltpu.VMEM((ctx, width), BF16),
            pltpu.VMEM(modw.shape, BF16),
            pltpu.VMEM((width, 384), BF16),
            pltpu.VMEM((2,) + wout.shape, BF16),
            pltpu.VMEM((latrows, 256), F32),
            pltpu.VMEM((nsp, 8, modcols), F32),
            pltpu.VMEM((ntp, 8, modcols), F32),
            pltpu.VMEM((ntp, padded, width), BF16),
            pltpu.VMEM((ctx, width), BF16),
            pltpu.VMEM((nsp, block_rows, 256), BF16),
            pltpu.VMEM((2, latrows, 128), BF16),
            pltpu.VMEM((latrows, 128), BF16),
            pltpu.VMEM((3, zn, padded, 128), BF16),
            pltpu.VMEM((zn, padded, width), BF16),
            pltpu.VMEM((zn, padded, width), BF16),
            dma((8,)), dma((3, ntp)), dma((ntp,)), dma((nsp,)), dma((nsp,)), dma((ntp,)),
            dma((ntp,)), dma((2, nsp)), dma((2, nsp)), dma((2, nsp)), dma, dma((2,)), dma, dma,
            dma((zn,)), dma((zn,)),
        ],
        compiler_params=pltpu.CompilerParams(
            collective_id=0, has_side_effects=True, vmem_limit_bytes=60 * 1024 * 1024
        ),
    )(latent, context, condl, condc, modw, wq, wk, wv, wout, lam, table)


def solution(mesh):
    nsp, ntp = mesh.shape["sp"], mesh.shape["tp"]
    placed = (
        P(("sp", "tp"), None),
        P("sp", None),
        P("sp"),
        P("sp"),
        P("sp", "tp"),
        P(None, "tp"),
        P(None, "tp"),
        P(None, "tp"),
        P("tp", None),
        P("tp"),
    )
    return jax.shard_map(
        functools.partial(shards, nsp, ntp), mesh=mesh, in_specs=placed,
        out_specs=P(("sp", "tp"), None), check_vma=False,
    )
```

time: 154 us -> 55.3 us (0.36)
  blocking collectives: 132 us -> 0 us
  Pallas kernels: 0 us -> 52.9 us
  matrix products: 8.4 us -> 0 us
  other arithmetic: 4.88 us -> 0 us
  starting transfers between devices: 2.92 us -> 0 us
    all_gather x4 -> x0, blocking collectives: 77.2 us -> none  [the longest x1 32.9 us: shards(): piece = lax.all_gather(own_rows, 'tp', axis=0, tiled=True)]
    pallas_call x0 -> x1, Pallas kernels: none -> 52.9 us  [shards(): pl.pallas_call(functools.partial(kernel, nsp, ntp, rows, padded, ctx, wid...]
    unnamed x1 -> x0, blocking collectives: 46.5 us -> none
    psum x1 -> x0, blocking collectives: 8.52 us -> none  [shards(): summed = lax.psum(partial_mod, 'sp')]
    dot_general x9 -> x0, matrix products: 8.4 us -> none  [the longest x1 1.77 us: shards(): jnp.dot(own_context, w_value, preferred_element_type=jnp.float32)]
    reduce_sum x5 -> x0, other arithmetic: 3.58 us -> none  [the longest x2 2.59 us: modulate_rows(): jnp.mean(values * values, axis=-1, keepdims=True) + NORM_EPS]
    unnamed x1 -> x0, starting transfers between devices: 2.92 us -> none
  transfers between devices with their start and end apart: 1 -> 0, of which waited for: 1 -> 0; matrix products, arithmetic and copies ran while one was open for 0% -> 0% of each run, Pallas kernels for 0% -> 0%
where the time goes in v1:
time: 55.3 us; the launch traced here: 55.1 us
  Pallas kernels  52.9 us (96%)
  local copies, waits for them, and re-layouts  1.57 us (3%)
  between operations  0.66 us (1%)
    pallas_call x1, Pallas kernels, shards(): pl.pallas_call(functools.partial(kernel, nsp, ntp, rows, padded, ctx, wid...  52.9 us
    unnamed x1, local copies, waits for them, and re-layouts  1.57 us

profile of v1, /device:TPU:0, one launch (start us, length us, event | category | flops | bytes accessed | tf_op | source)
XLA Modules:
  0.0 55.1 jit_solution(5973219789882767725)
XLA Ops:
  0.7 52.9 %shard_map.109 = bf16[30,2048]{1,0:T(8,128)(2,1)} custom-call(bf16[30,2048]{1,0:T(8,128)(2,1)} %latent.1, bf16[192,2048]{1,0:T(8,128)(2,1)} %context.1, f32[512]{0:T(512)} %condl.1, f32[512]{0:T(512)} %condc.1, bf16[512,768]{1,0:T(8,128)(2,1)} %modw.1, bf16[2048,128]{1,0:T(8,128)(2,1)} %wq.1, bf16[2048,128]{1,0:T(8,128)(2,1)} %wk.1, bf16[2048,128]{1,0:T(8,128)(2,1)} %wv.1, ...), custom_call_target="tpu_custom_call" | custom-call | tf_op jit(solution)/shard_map/pallas_call | solution.py:359
  53.5 1.6 %copy.14 = bf16[30,2048]{1,0:T(8,128)(2,1)} copy(bf16[30,2048]{1,0:T(8,128)(2,1)} %shard_map.109) | data formatting | bytes 245760

commit v2 on v1

--- a/solution.py
+++ b/solution.py
@@ -16,6 +16,7 @@
 THETA = 10000.0
 F32 = jnp.float32
 BF16 = jnp.bfloat16
+NCH = 4
 
 
 def rotary_tables(nsp, ntp, rows, padded):
@@ -29,14 +30,15 @@
     both = np.concatenate([np.cos(angle), np.sin(angle) * sign], axis=-1).astype(np.float32)
     full = np.zeros((nsp * ntp, padded, 4 * QK_DIM), np.float32)
     full[:, :rows] = both.reshape(nsp * ntp, rows, -1)
-    return full.reshape(nsp, ntp * padded, -1)
+    full = full.reshape(nsp, ntp // 2, 2, padded, -1).transpose(0, 2, 1, 3, 4)
+    return np.ascontiguousarray(full).reshape(nsp, 2, ntp // 2 * padded, -1)
 
 
 def kernel(
     nsp, ntp, rows, padded, ctx, width, modcols, qb,
     latent, context, condl, condc, modw, wq, wk, wv, wout, lam, table,
     out,
-    raw, ctxv, modwv, wcat, wo, tab, part, mods, nbuf, nctx, kv, qbuf, att, att2, send, outb,
+    raw, ctxv, modwv, wcat, wo, tab, part, mods, nbuf, nctx, kv, qbuf, att, attx, send, outb,
     loc, rsend, rrecv, p1s, p1r, p2s, p2r, kvs, kvf, kvr, ws, wr, ats, atr, os, orr,
 ):
     sp, tp = lax.axis_index("sp"), lax.axis_index("tp")
@@ -46,7 +48,9 @@
     xpeer = zi * 2 + (1 - xi)
     cpeer = yi * 2 + (1 - ci)
     latrows = ntp * padded
+    half = zn * padded
     block_rows = latrows + ctx
+    chunk = width // NCH
 
     def local(i, src, dst):
         return pltpu.make_async_copy(src, dst, loc.at[i])
@@ -64,8 +68,9 @@
         local(3, wk, wcat.at[:, pl.ds(0, 128)]),
         local(4, wv, wcat.at[:, pl.ds(128, 128)]),
         local(5, wq, wcat.at[:, pl.ds(256, 128)]),
-        local(6, table.at[sp], tab),
+        local(6, table.at[sp, xi], tab.at[0]),
         local(7, wout, wo.at[xi]),
+        local(8, table.at[sp, 1 - xi], tab.at[1]),
     ]
     for c in copies:
         c.start()
@@ -85,6 +90,57 @@
             barrier, inc=1, device_id=(lax.rem(sp + d, nsp), tp),
             device_id_type=pl.DeviceIdType.MESH,
         )
+
+    copies[0].wait()
+    pl.semaphore_wait(barrier, (ntp - 1) + (nsp - 1))
+
+    def row_copy(way, t, c, to):
+        cols = pl.ds(c * chunk, chunk)
+        return remote(
+            raw.at[t, :, cols], raw.at[t, :, cols], rsend.at[way, t, c], rrecv.at[t, c], sp, to
+        )
+
+    def up(t, c):
+        return row_copy(0, t, c, lax.rem(tp + 2, ntp))
+
+    def down(t, c):
+        return row_copy(1, t, c, lax.rem(tp + ntp - 2, ntp))
+
+    def across(t, c):
+        return row_copy(2, t, c, xpeer)
+
+    def forward(t, c, from_below):
+        if from_below is not False:
+
+            @pl.when(zi < zn - 1)
+            def _():
+                up(t, c).start()
+
+        if from_below is not True:
+
+            @pl.when(zi > 0)
+            def _():
+                down(t, c).start()
+
+        across(t, c).start()
+
+    for c in range(NCH):
+        forward(tp, c, None)
+
+    def row_step(s):
+        for c in range(NCH):
+
+            @pl.when(zi - s >= 0)
+            def _():
+                t = tp - 2 * s
+                across(t, c).wait_recv()
+                forward(t, c, True)
+
+            @pl.when(zi + s < zn)
+            def _():
+                t = tp + 2 * s
+                across(t, c).wait_recv()
+                forward(t, c, False)
 
     copies[1].wait()
     cl = jax.nn.silu(condl[...]).reshape(1, -1)
@@ -92,58 +148,12 @@
     row = lax.broadcasted_iota(jnp.int32, (8, cl.shape[1]), 0)
     cond = jnp.where(row == 0, cl, jnp.where(row == 1, cc, 0.0)).astype(BF16)
     part[sp] = jnp.dot(cond, modwv[...], preferred_element_type=F32)
-    copies[0].wait()
-    pl.semaphore_wait(barrier, (ntp - 1) + (nsp - 1))
-
     def p1(d, src):
         return remote(part.at[src], part.at[src], p1s.at[d], p1r.at[src], lax.rem(sp + d, nsp), tp)
 
     @pl.loop(1, nsp)
     def _(d):
         p1(d, sp).start()
-
-    def row_copy(way, t, to):
-        return remote(raw.at[t], raw.at[t], rsend.at[way, t], rrecv.at[t], sp, to)
-
-    def up(t):
-        return row_copy(0, t, lax.rem(tp + 2, ntp))
-
-    def down(t):
-        return row_copy(1, t, lax.rem(tp + ntp - 2, ntp))
-
-    def across(t):
-        return row_copy(2, t, xpeer)
-
-    def forward(t, from_below):
-        if from_below is not False:
-
-            @pl.when(zi < zn - 1)
-            def _():
-                up(t).start()
-
-        if from_below is not True:
-
-            @pl.when(zi > 0)
-            def _():
-                down(t).start()
-
-        across(t).start()
-
-    forward(tp, None)
-    copies[7].wait()
-
-    def row_step(s):
-        @pl.when(zi - s >= 0)
-        def _():
-            t = tp - 2 * s
-            across(t).wait_recv()
-            forward(t, True)
-
-        @pl.when(zi + s < zn)
-        def _():
-            t = tp + 2 * s
-            across(t).wait_recv()
-            forward(t, False)
 
     @pl.loop(1, nsp)
     def _(d):
@@ -162,6 +172,8 @@
         p2(d, tp).start()
 
     row_step(1)
+    if zn > 2:
+        row_step(2)
 
     @pl.loop(1, ntp)
     def _(d):
@@ -181,20 +193,20 @@
     nctx[...] = normed(ctxv[...], scale_c, shift_c)
     copies[3].wait()
     copies[4].wait()
-    lat_part, ctx_part = pl.ds(0, latrows), pl.ds(latrows, ctx)
+    pieces = (pl.ds(0, half), pl.ds(half, half), pl.ds(latrows, ctx))
     kv[sp, latrows:block_rows, :] = jnp.dot(
         nctx[...], wcat[:, 0:256], preferred_element_type=F32
     ).astype(BF16)
 
     def kv_direct(which, d, src):
-        piece = (lat_part, ctx_part)[which]
+        piece = pieces[which]
         return remote(
             kv.at[src, piece], kv.at[src, piece], kvs.at[which, d], kvr.at[which, src],
             lax.rem(sp + 2 * d, nsp), tp,
         )
 
     def kv_forward(which, src):
-        piece = (lat_part, ctx_part)[which]
+        piece = pieces[which]
         return remote(
             kv.at[src, piece], kv.at[src, piece], kvf.at[which, src], kvr.at[which, src], cpeer, tp
         )
@@ -214,46 +226,52 @@
         for y in range(yn):
             kv_forward(which, y * 2 + (1 - ci)).wait_recv()
 
-    kv_send(1)
-    for s in range(2, zn):
+    kv_send(2)
+    for s in range(3, zn):
         row_step(s)
+    copies[7].wait()
     wo_copy = remote(wo.at[xi], wo.at[xi], ws, wr.at[xi], sp, xpeer)
     wo_copy.start()
-    kv_relay(1)
-
     nbuf[...] = jnp.zeros_like(nbuf)
 
-    def norm_row(t):
-        nbuf[t, 0:rows, :] = normed(raw[t], scale_l, shift_l)
-
-    for z in range(zn):
-        norm_row(z * 2 + xi)
-    for z in range(zn):
-        t = z * 2 + (1 - xi)
-        across(t).wait_recv()
-        norm_row(t)
-    copies[5].wait()
-    copies[6].wait()
-    x = nbuf[...].reshape(latrows, width)
-    pkv = jnp.dot(x, wcat[:, 0:256], preferred_element_type=F32)
-    cosine, sine = tab[:, 0:128], tab[:, 128:256]
     quarter = QK_DIM // 4
     lane = lax.broadcasted_iota(jnp.int32, (1, 128), 1)
     low = lax.rem(lane, 2 * quarter) < quarter
 
-    def rotate(u):
+    def rotate(u, k):
         turned = jnp.where(low, pltpu.roll(u, 128 - quarter, 1), pltpu.roll(u, quarter, 1))
-        return (u * cosine + turned * sine).astype(BF16)
-
-    kv[sp, 0:latrows, 0:128] = rotate(pkv[:, 0:128])
-    kv[sp, 0:latrows, 128:256] = pkv[:, 128:256].astype(BF16)
-    kv_send(0)
-    q = rotate(jnp.dot(x, wcat[:, 256:384], preferred_element_type=F32)) * BF16(QK_DIM**-0.5)
-    qbuf[0] = jnp.where(lane < QK_DIM, q, BF16(0))
-    qbuf[1] = jnp.where(lane < QK_DIM, BF16(0), q)
+        return (u * tab[k, :, 0:128] + turned * tab[k, :, 128:256]).astype(BF16)
+
+    def project(k):
+        x = nbuf[k * zn : (k + 1) * zn].reshape(half, width)
+        pkv = jnp.dot(x, wcat[:, 0:256], preferred_element_type=F32)
+        here = slice(k * half, (k + 1) * half)
+        kv[sp, here, 0:128] = rotate(pkv[:, 0:128], k)
+        kv[sp, here, 128:256] = pkv[:, 128:256].astype(BF16)
+        kv_send(k)
+        q = jnp.dot(x, wcat[:, 256:384], preferred_element_type=F32)
+        q = rotate(q, k) * BF16(QK_DIM**-0.5)
+        qbuf[0, here, :] = jnp.where(lane < QK_DIM, q, BF16(0))
+        qbuf[1, here, :] = jnp.where(lane < QK_DIM, BF16(0), q)
+
+    for z in range(zn):
+        nbuf[z, 0:rows, :] = normed(raw[z * 2 + xi], scale_l, shift_l)
+    copies[5].wait()
+    copies[6].wait()
+    copies[8].wait()
+    project(0)
+    kv_relay(2)
+    for z in range(zn):
+        t = z * 2 + (1 - xi)
+        for c in range(NCH):
+            across(t, c).wait_recv()
+        nbuf[zn + z, 0:rows, :] = normed(raw[t], scale_l, shift_l)
     kv_relay(0)
+    project(1)
+    kv_relay(1)
+    kv_finish(2)
+    kv_finish(0)
     kv_finish(1)
-    kv_finish(0)
 
     keys = nsp * block_rows
     col = lax.rem(lax.broadcasted_iota(jnp.int32, (1, keys), 1), block_rows)
@@ -261,8 +279,7 @@
     bias = jnp.where(empty, F32(-1e30), F32(0.0))
     factor = lam[0]
 
-    @pl.loop(0, latrows // qb)
-    def _(i):
+    def attend(i):
         here = pl.ds(pl.multiple_of(i * qb, qb), qb)
         mixed = []
         for m in range(2):
@@ -280,11 +297,10 @@
         h = h * lax.rsqrt(jnp.mean(h * h, axis=-1, keepdims=True) + HEAD_EPS)
         att[here, :] = h.astype(BF16)
 
-    for z in range(zn):
-        for x01 in range(2):
-            att2[x01, z] = att[(z * 2 + x01) * padded : (z * 2 + x01 + 1) * padded, :]
-    at_copy = remote(att2.at[1 - xi], att2.at[2], ats, atr, sp, xpeer)
+    pl.loop(half // qb, latrows // qb)(attend)
+    at_copy = remote(att.at[pl.ds(half, half)], attx, ats, atr, sp, xpeer)
     at_copy.start()
+    pl.loop(0, half // qb)(attend)
     remote(wo.at[1 - xi], wo.at[1 - xi], ws, wr.at[1 - xi], sp, xpeer).wait_recv()
     at_copy.wait_recv()
     w_mine, w_other = wo[xi], wo[1 - xi]
@@ -295,8 +311,9 @@
 
     for d in range(zn - 1, -1, -1):
         z = lax.rem(zi + d, zn)
-        y = jnp.dot(att2[xi, z], w_mine, preferred_element_type=F32) + jnp.dot(
-            att2[2, z], w_other, preferred_element_type=F32
+        here = pl.ds(pl.multiple_of(z * padded, padded), padded)
+        y = jnp.dot(att[here, :], w_mine, preferred_element_type=F32) + jnp.dot(
+            attx[here, :], w_other, preferred_element_type=F32
         )
         if d:
             send[d] = y.astype(BF16)
@@ -318,18 +335,19 @@
         p2(d, tp).wait_send()
 
     for z in range(zn):
-        t = z * 2 + xi
-
-        @pl.when(jnp.logical_and(z <= zi, zi < zn - 1))
-        def _():
-            up(t).wait_send()
-
-        @pl.when(jnp.logical_and(z >= zi, zi > 0))
-        def _():
-            down(t).wait_send()
-
-        across(t).wait_send()
-    for which in range(2):
+        for c in range(NCH):
+            t = z * 2 + xi
+
+            @pl.when(jnp.logical_and(z <= zi, zi < zn - 1))
+            def _():
+                up(t, c).wait_send()
+
+            @pl.when(jnp.logical_and(z >= zi, zi > 0))
+            def _():
+                down(t, c).wait_send()
+
+            across(t, c).wait_send()
+    for which in range(3):
         for d in range(1, yn):
             kv_direct(which, d, sp).wait_send()
         for y in range(yn):
@@ -348,7 +366,7 @@
     block_rows = latrows + ctx
     modcols = modw.shape[1]
     zn = ntp // 2
-    qb = latrows
+    qb = latrows // 2
     while qb % 32 == 0 and qb * nsp * block_rows * 4 > 1_000_000:
         qb //= 2
     table = jnp.asarray(rotary_tables(nsp, ntp, rows, padded))
@@ -367,7 +385,7 @@
             pltpu.VMEM(modw.shape, BF16),
             pltpu.VMEM((width, 384), BF16),
             pltpu.VMEM((2,) + wout.shape, BF16),
-            pltpu.VMEM((latrows, 256), F32),
+            pltpu.VMEM((2, latrows // 2, 256), F32),
             pltpu.VMEM((nsp, 8, modcols), F32),
             pltpu.VMEM((ntp, 8, modcols), F32),
             pltpu.VMEM((ntp, padded, width), BF16),
@@ -375,11 +393,11 @@
             pltpu.VMEM((nsp, block_rows, 256), BF16),
             pltpu.VMEM((2, latrows, 128), BF16),
             pltpu.VMEM((latrows, 128), BF16),
-            pltpu.VMEM((3, zn, padded, 128), BF16),
+            pltpu.VMEM((latrows // 2, 128), BF16),
             pltpu.VMEM((zn, padded, width), BF16),
             pltpu.VMEM((zn, padded, width), BF16),
-            dma((8,)), dma((3, ntp)), dma((ntp,)), dma((nsp,)), dma((nsp,)), dma((ntp,)),
-            dma((ntp,)), dma((2, nsp)), dma((2, nsp)), dma((2, nsp)), dma, dma((2,)), dma, dma,
+            dma((9,)), dma((3, ntp, NCH)), dma((ntp, NCH)), dma((nsp,)), dma((nsp,)), dma((ntp,)),
+            dma((ntp,)), dma((3, nsp)), dma((3, nsp)), dma((3, nsp)), dma, dma((2,)), dma, dma,
             dma((zn,)), dma((zn,)),
         ],
         compiler_params=pltpu.CompilerParams(

time: 55.3 us -> 52.8 us (0.955)
  Pallas kernels: 52.9 us -> 50.4 us
    pallas_call x1, Pallas kernels: 52.9 us -> 50.4 us  [shards(): pl.pallas_call(functools.partial(kernel, nsp, ntp, rows, padded, ctx, wid...]
where the time goes in v2:
time: 52.8 us; the launch traced here: 52.6 us
  Pallas kernels  50.4 us (95%)
  local copies, waits for them, and re-layouts  1.57 us (3%)
  between operations  0.66 us (1%)
    pallas_call x1, Pallas kernels, shards(): pl.pallas_call(functools.partial(kernel, nsp, ntp, rows, padded, ctx, wid...  50.4 us
    unnamed x1, local copies, waits for them, and re-layouts  1.57 us

profile of v2, /device:TPU:0, one launch (start us, length us, event | category | flops | bytes accessed | tf_op | source)
XLA Modules:
  0.0 52.6 jit_solution(7380751211130638400)
XLA Ops:
  0.7 50.4 %shard_map.109 = bf16[30,2048]{1,0:T(8,128)(2,1)} custom-call(bf16[30,2048]{1,0:T(8,128)(2,1)} %latent.1, bf16[192,2048]{1,0:T(8,128)(2,1)} %context.1, f32[512]{0:T(512)} %condl.1, f32[512]{0:T(512)} %condc.1, bf16[512,768]{1,0:T(8,128)(2,1)} %modw.1, bf16[2048,128]{1,0:T(8,128)(2,1)} %wq.1, bf16[2048,128]{1,0:T(8,128)(2,1)} %wk.1, bf16[2048,128]{1,0:T(8,128)(2,1)} %wv.1, ...), custom_call_target="tpu_custom_call" | custom-call | tf_op jit(solution)/shard_map/pallas_call | solution.py:377
  51.0 1.6 %copy.14 = bf16[30,2048]{1,0:T(8,128)(2,1)} copy(bf16[30,2048]{1,0:T(8,128)(2,1)} %shard_map.109) | data formatting | bytes 245760

commit v3 on v2

--- a/solution.py
+++ b/solution.py
@@ -30,8 +30,8 @@
     both = np.concatenate([np.cos(angle), np.sin(angle) * sign], axis=-1).astype(np.float32)
     full = np.zeros((nsp * ntp, padded, 4 * QK_DIM), np.float32)
     full[:, :rows] = both.reshape(nsp * ntp, rows, -1)
-    full = full.reshape(nsp, ntp // 2, 2, padded, -1).transpose(0, 2, 1, 3, 4)
-    return np.ascontiguousarray(full).reshape(nsp, 2, ntp // 2 * padded, -1)
+    full = full.reshape(nsp, ntp // 4, 2, 2, padded, -1).transpose(0, 3, 2, 1, 4, 5)
+    return np.ascontiguousarray(full).reshape(nsp, 2, 2, ntp // 4 * padded, -1)
 
 
 def kernel(
@@ -49,8 +49,14 @@
     cpeer = yi * 2 + (1 - ci)
     latrows = ntp * padded
     half = zn * padded
+    nq = zn // 2
+    quart = nq * padded
+    ki, pz = zi // 2, lax.rem(zi, 2)
+    zpeer = (ki * 2 + 1 - pz) * 2 + xi
+    xzpeer = (ki * 2 + 1 - pz) * 2 + 1 - xi
     block_rows = latrows + ctx
     chunk = width // NCH
+    hw = wo.shape[1] // 2
 
     def local(i, src, dst):
         return pltpu.make_async_copy(src, dst, loc.at[i])
@@ -68,9 +74,11 @@
         local(3, wk, wcat.at[:, pl.ds(0, 128)]),
         local(4, wv, wcat.at[:, pl.ds(128, 128)]),
         local(5, wq, wcat.at[:, pl.ds(256, 128)]),
-        local(6, table.at[sp, xi], tab.at[0]),
-        local(7, wout, wo.at[xi]),
-        local(8, table.at[sp, 1 - xi], tab.at[1]),
+        local(6, table.at[sp, xi, pz], tab.at[0, pl.ds(0, quart)]),
+        local(7, wout, wo.at[0]),
+        local(8, table.at[sp, 1 - xi, pz], tab.at[1, pl.ds(0, quart)]),
+        local(9, table.at[sp, xi, 1 - pz], tab.at[0, pl.ds(quart, quart)]),
+        local(10, table.at[sp, 1 - xi, 1 - pz], tab.at[1, pl.ds(quart, quart)]),
     ]
     for c in copies:
         c.start()
@@ -230,8 +238,23 @@
     for s in range(3, zn):
         row_step(s)
     copies[7].wait()
-    wo_copy = remote(wo.at[xi], wo.at[xi], ws, wr.at[xi], sp, xpeer)
-    wo_copy.start()
+    mine = pl.ds(pl.multiple_of(ci * hw, hw), hw)
+
+    def wo_copy(i, src, dst, to_sp, to_tp, core):
+        return remote(wo.at[src, mine], wo.at[dst, mine], ws.at[i], wr.at[dst, core], to_sp, to_tp)
+
+    wo_z = wo_copy(0, 0, 1, sp, zpeer, ci)
+    wo_x = wo_copy(1, 0, 2, sp, xpeer, ci)
+    wo_xz = wo_copy(2, 1, 3, sp, xpeer, ci)
+    wo_core = [wo_copy(2 + r, r, r, cpeer, tp, ci) for r in range(1, 4)]
+
+    def wo_arrival(r):
+        other = pl.ds(pl.multiple_of((1 - ci) * hw, hw), hw)
+        return remote(wo.at[r, other], wo.at[r, other], ws.at[2 + r], wr.at[r, 1 - ci], cpeer, tp)
+
+    wo_z.start()
+    wo_x.start()
+
     nbuf[...] = jnp.zeros_like(nbuf)
 
     quarter = QK_DIM // 4
@@ -254,20 +277,27 @@
         qbuf[0, here, :] = jnp.where(lane < QK_DIM, q, BF16(0))
         qbuf[1, here, :] = jnp.where(lane < QK_DIM, BF16(0), q)
 
-    for z in range(zn):
-        nbuf[z, 0:rows, :] = normed(raw[z * 2 + xi], scale_l, shift_l)
+    def position(i):
+        return 2 * (i % nq) + (pz if i < nq else 1 - pz)
+
+    for i in range(zn):
+        nbuf[i, 0:rows, :] = normed(raw[position(i) * 2 + xi], scale_l, shift_l)
     copies[5].wait()
     copies[6].wait()
-    copies[8].wait()
+    for i in range(8, 11):
+        copies[i].wait()
     project(0)
     kv_relay(2)
-    for z in range(zn):
-        t = z * 2 + (1 - xi)
+    for i in range(zn):
+        t = position(i) * 2 + (1 - xi)
         for c in range(NCH):
             across(t, c).wait_recv()
-        nbuf[zn + z, 0:rows, :] = normed(raw[t], scale_l, shift_l)
+        nbuf[zn + i, 0:rows, :] = normed(raw[t], scale_l, shift_l)
     kv_relay(0)
     project(1)
+    wo_z.wait_recv()
+    wo_xz.start()
+    wo_core[0].start()
     kv_relay(1)
     kv_finish(2)
     kv_finish(0)
@@ -298,29 +328,39 @@
         att[here, :] = h.astype(BF16)
 
     pl.loop(half // qb, latrows // qb)(attend)
-    at_copy = remote(att.at[pl.ds(half, half)], attx, ats, atr, sp, xpeer)
-    at_copy.start()
+    def at_copy(r, to):
+        return remote(
+            att.at[pl.ds(r * quart, quart)], attx.at[:, pl.ds(r * 128, 128)],
+            ats.at[r], atr.at[r], sp, to,
+        )
+
+    at = [None, at_copy(1, zpeer), at_copy(2, xpeer), at_copy(3, xzpeer)]
+    at[3].start()
+    at[2].start()
+    wo_x.wait_recv()
+    wo_core[1].start()
     pl.loop(0, half // qb)(attend)
-    remote(wo.at[1 - xi], wo.at[1 - xi], ws, wr.at[1 - xi], sp, xpeer).wait_recv()
-    at_copy.wait_recv()
-    w_mine, w_other = wo[xi], wo[1 - xi]
+    at[1].start()
+    attx[:, 0:128] = att[0:quart, :]
+    wo_xz.wait_recv()
+    wo_core[2].start()
+    for r in range(1, 4):
+        wo_arrival(r).wait_recv()
+        at[r].wait_recv()
+    w_all = wo[...].reshape(4 * wo.shape[1], width)
 
     def out_copy(d, src):
-        to = lax.rem(zi + d, zn) * 2 + xi
+        to = (2 * lax.rem(ki + d, nq) + pz) * 2 + xi
         return remote(send.at[d], outb.at[src], os.at[d], orr.at[src], sp, to)
 
-    for d in range(zn - 1, -1, -1):
-        z = lax.rem(zi + d, zn)
-        here = pl.ds(pl.multiple_of(z * padded, padded), padded)
-        y = jnp.dot(att[here, :], w_mine, preferred_element_type=F32) + jnp.dot(
-            attx[here, :], w_other, preferred_element_type=F32
-        )
+    for d in range(nq - 1, -1, -1):
+        here = pl.ds(pl.multiple_of(lax.rem(ki + d, nq) * padded, padded), padded)
+        branch = jnp.dot(attx[here, :], w_all, preferred_element_type=F32)
         if d:
-            send[d] = y.astype(BF16)
-            out_copy(d, zi).start()
-    branch = y
-    for d in range(1, zn):
-        src = lax.rem(zi + zn - d, zn)
+            send[d] = branch.astype(BF16)
+            out_copy(d, ki).start()
+    for d in range(1, nq):
+        src = lax.rem(ki + nq - d, nq)
         out_copy(d, src).wait_recv()
         branch = branch + outb[src].astype(F32)
     branch = branch * lax.rsqrt(jnp.mean(branch * branch, axis=-1, keepdims=True) + NORM_EPS)
@@ -352,10 +392,10 @@
             kv_direct(which, d, sp).wait_send()
         for y in range(yn):
             kv_forward(which, y * 2 + ci).wait_send()
-    wo_copy.wait_send()
-    at_copy.wait_send()
-    for d in range(1, zn):
-        out_copy(d, zi).wait_send()
+    for c in [wo_z, wo_x, wo_xz] + wo_core + at[1:]:
+        c.wait_send()
+    for d in range(1, nq):
+        out_copy(d, ki).wait_send()
 
 
 def shards(nsp, ntp, latent, context, condl, condc, modw, wq, wk, wv, wout, lam):
@@ -384,7 +424,7 @@
             pltpu.VMEM((ctx, width), BF16),
             pltpu.VMEM(modw.shape, BF16),
             pltpu.VMEM((width, 384), BF16),
-            pltpu.VMEM((2,) + wout.shape, BF16),
+            pltpu.VMEM((4,) + wout.shape, BF16),
             pltpu.VMEM((2, latrows // 2, 256), F32),
             pltpu.VMEM((nsp, 8, modcols), F32),
             pltpu.VMEM((ntp, 8, modcols), F32),
@@ -393,12 +433,12 @@
             pltpu.VMEM((nsp, block_rows, 256), BF16),
             pltpu.VMEM((2, latrows, 128), BF16),
             pltpu.VMEM((latrows, 128), BF16),
-            pltpu.VMEM((latrows // 2, 128), BF16),
-            pltpu.VMEM((zn, padded, width), BF16),
-            pltpu.VMEM((zn, padded, width), BF16),
-            dma((9,)), dma((3, ntp, NCH)), dma((ntp, NCH)), dma((nsp,)), dma((nsp,)), dma((ntp,)),
-            dma((ntp,)), dma((3, nsp)), dma((3, nsp)), dma((3, nsp)), dma, dma((2,)), dma, dma,
-            dma((zn,)), dma((zn,)),
+            pltpu.VMEM((latrows // 4, 512), BF16),
+            pltpu.VMEM((zn // 2, padded, width), BF16),
+            pltpu.VMEM((zn // 2, padded, width), BF16),
+            dma((11,)), dma((3, ntp, NCH)), dma((ntp, NCH)), dma((nsp,)), dma((nsp,)), dma((ntp,)),
+            dma((ntp,)), dma((3, nsp)), dma((3, nsp)), dma((3, nsp)), dma((6,)), dma((4, 2)), dma((4,)), dma((4,)),
+            dma((zn // 2,)), dma((zn // 2,)),
         ],
         compiler_params=pltpu.CompilerParams(
             collective_id=0, has_side_effects=True, vmem_limit_bytes=60 * 1024 * 1024

time: 52.8 us -> 49.9 us (0.945)
  Pallas kernels: 50.4 us -> 47.4 us
    pallas_call x1, Pallas kernels: 50.4 us -> 47.4 us  [shards(): pl.pallas_call(functools.partial(kernel, nsp, ntp, rows, padded, ctx, wid...]
where the time goes in v3:
time: 49.9 us; the launch traced here: 49.7 us
  Pallas kernels  47.4 us (95%)
  local copies, waits for them, and re-layouts  1.57 us (3%)
  between operations  0.66 us (1%)
    pallas_call x1, Pallas kernels, shards(): pl.pallas_call(functools.partial(kernel, nsp, ntp, rows, padded, ctx, wid...  47.4 us
    unnamed x1, local copies, waits for them, and re-layouts  1.57 us

profile of v3, /device:TPU:0, one launch (start us, length us, event | category | flops | bytes accessed | tf_op | source)
XLA Modules:
  0.0 49.7 jit_solution(8415394760999194234)
XLA Ops:
  0.7 47.4 %shard_map.109 = bf16[30,2048]{1,0:T(8,128)(2,1)} custom-call(bf16[30,2048]{1,0:T(8,128)(2,1)} %latent.1, bf16[192,2048]{1,0:T(8,128)(2,1)} %context.1, f32[512]{0:T(512)} %condl.1, f32[512]{0:T(512)} %condc.1, bf16[512,768]{1,0:T(8,128)(2,1)} %modw.1, bf16[2048,128]{1,0:T(8,128)(2,1)} %wq.1, bf16[2048,128]{1,0:T(8,128)(2,1)} %wk.1, bf16[2048,128]{1,0:T(8,128)(2,1)} %wv.1, ...), custom_call_target="tpu_custom_call" | custom-call | tf_op jit(solution)/shard_map/pallas_call | solution.py:417
  48.1 1.6 %copy.14 = bf16[30,2048]{1,0:T(8,128)(2,1)} copy(bf16[30,2048]{1,0:T(8,128)(2,1)} %shard_map.109) | data formatting | bytes 245760

commit v4 on v3

--- a/solution.py
+++ b/solution.py
@@ -105,7 +105,7 @@
     def row_copy(way, t, c, to):
         cols = pl.ds(c * chunk, chunk)
         return remote(
-            raw.at[t, :, cols], raw.at[t, :, cols], rsend.at[way, t, c], rrecv.at[t, c], sp, to
+            raw.at[t, :, cols], raw.at[t, :, cols], rsend.at[way, t // 2], rrecv.at[t, c], sp, to
         )
 
     def up(t, c):
@@ -155,7 +155,7 @@
     cc = jax.nn.silu(condc[...]).reshape(1, -1)
     row = lax.broadcasted_iota(jnp.int32, (8, cl.shape[1]), 0)
     cond = jnp.where(row == 0, cl, jnp.where(row == 1, cc, 0.0)).astype(BF16)
-    part[sp] = jnp.dot(cond, modwv[...], preferred_element_type=F32)
+    part[sp] = jnp.dot(cond, modwv[...], preferred_element_type=F32)[0:2]
     def p1(d, src):
         return remote(part.at[src], part.at[src], p1s.at[d], p1r.at[src], lax.rem(sp + d, nsp), tp)
 
@@ -182,6 +182,23 @@
     row_step(1)
     if zn > 2:
         row_step(2)
+
+    mine = pl.ds(pl.multiple_of(ci * hw, hw), hw)
+
+    def wo_copy(i, src, dst, to_sp, to_tp, core):
+        return remote(wo.at[src, mine], wo.at[dst, mine], ws.at[i], wr.at[dst, core], to_sp, to_tp)
+
+    wo_z = wo_copy(0, 0, 1, sp, zpeer, ci)
+    wo_x = wo_copy(1, 0, 2, sp, xpeer, ci)
+    wo_xz = wo_copy(2, 1, 3, sp, xpeer, ci)
+    wo_core = [wo_copy(2 + r, r, r, cpeer, tp, ci) for r in range(1, 4)]
+
+    def wo_arrival(r):
+        other = pl.ds(pl.multiple_of((1 - ci) * hw, hw), hw)
+        return remote(wo.at[r, other], wo.at[r, other], ws.at[2 + r], wr.at[r, 1 - ci], cpeer, tp)
+
+    copies[7].wait()
+    wo_z.start()
 
     @pl.loop(1, ntp)
     def _(d):
@@ -237,22 +254,6 @@
     kv_send(2)
     for s in range(3, zn):
         row_step(s)
-    copies[7].wait()
-    mine = pl.ds(pl.multiple_of(ci * hw, hw), hw)
-
-    def wo_copy(i, src, dst, to_sp, to_tp, core):
-        return remote(wo.at[src, mine], wo.at[dst, mine], ws.at[i], wr.at[dst, core], to_sp, to_tp)
-
-    wo_z = wo_copy(0, 0, 1, sp, zpeer, ci)
-    wo_x = wo_copy(1, 0, 2, sp, xpeer, ci)
-    wo_xz = wo_copy(2, 1, 3, sp, xpeer, ci)
-    wo_core = [wo_copy(2 + r, r, r, cpeer, tp, ci) for r in range(1, 4)]
-
-    def wo_arrival(r):
-        other = pl.ds(pl.multiple_of((1 - ci) * hw, hw), hw)
-        return remote(wo.at[r, other], wo.at[r, other], ws.at[2 + r], wr.at[r, 1 - ci], cpeer, tp)
-
-    wo_z.start()
     wo_x.start()
 
     nbuf[...] = jnp.zeros_like(nbuf)
@@ -274,8 +275,12 @@
         kv_send(k)
         q = jnp.dot(x, wcat[:, 256:384], preferred_element_type=F32)
         q = rotate(q, k) * BF16(QK_DIM**-0.5)
-        qbuf[0, here, :] = jnp.where(lane < QK_DIM, q, BF16(0))
-        qbuf[1, here, :] = jnp.where(lane < QK_DIM, BF16(0), q)
+        for i in range(zn):
+            u = q[i * padded : (i + 1) * padded]
+            d = lax.rem(i % nq + nq - ki, nq)
+            to = pl.ds(pl.multiple_of((d * 4 + k * 2 + i // nq) * padded, padded), padded)
+            qbuf[0, to, :] = jnp.where(lane < QK_DIM, u, BF16(0))
+            qbuf[1, to, :] = jnp.where(lane < QK_DIM, BF16(0), u)
 
     def position(i):
         return 2 * (i % nq) + (pz if i < nq else 1 - pz)
@@ -287,6 +292,9 @@
     for i in range(8, 11):
         copies[i].wait()
     project(0)
+    wo_z.wait_recv()
+    wo_xz.start()
+    wo_core[0].start()
     kv_relay(2)
     for i in range(zn):
         t = position(i) * 2 + (1 - xi)
@@ -295,9 +303,6 @@
         nbuf[zn + i, 0:rows, :] = normed(raw[t], scale_l, shift_l)
     kv_relay(0)
     project(1)
-    wo_z.wait_recv()
-    wo_xz.start()
-    wo_core[0].start()
     kv_relay(1)
     kv_finish(2)
     kv_finish(0)
@@ -327,26 +332,29 @@
         h = h * lax.rsqrt(jnp.mean(h * h, axis=-1, keepdims=True) + HEAD_EPS)
         att[here, :] = h.astype(BF16)
 
-    pl.loop(half // qb, latrows // qb)(attend)
-    def at_copy(r, to):
+    group = 4 * padded
+
+    def at_copy(d, r, to):
         return remote(
-            att.at[pl.ds(r * quart, quart)], attx.at[:, pl.ds(r * 128, 128)],
-            ats.at[r], atr.at[r], sp, to,
-        )
-
-    at = [None, at_copy(1, zpeer), at_copy(2, xpeer), at_copy(3, xzpeer)]
-    at[3].start()
-    at[2].start()
+            att.at[pl.ds(d * group + r * padded, padded)], attx.at[d, :, pl.ds(r * 128, 128)],
+            ats.at[d, r], atr.at[d, r], sp, to,
+        )
+
+    def attended(d):
+        pl.loop(d * (group // qb), (d + 1) * (group // qb))(attend)
+        attx[d, :, 0:128] = att[d * group : d * group + padded, :]
+        for r, to in ((3, xzpeer), (2, xpeer), (1, zpeer)):
+            at_copy(d, r, to).start()
+
+    attended(nq - 1)
     wo_x.wait_recv()
     wo_core[1].start()
-    pl.loop(0, half // qb)(attend)
-    at[1].start()
-    attx[:, 0:128] = att[0:quart, :]
+    for d in range(nq - 2, -1, -1):
+        attended(d)
     wo_xz.wait_recv()
     wo_core[2].start()
     for r in range(1, 4):
         wo_arrival(r).wait_recv()
-        at[r].wait_recv()
     w_all = wo[...].reshape(4 * wo.shape[1], width)
 
     def out_copy(d, src):
@@ -354,8 +362,9 @@
         return remote(send.at[d], outb.at[src], os.at[d], orr.at[src], sp, to)
 
     for d in range(nq - 1, -1, -1):
-        here = pl.ds(pl.multiple_of(lax.rem(ki + d, nq) * padded, padded), padded)
-        branch = jnp.dot(attx[here, :], w_all, preferred_element_type=F32)
+        for r in range(1, 4):
+            at_copy(d, r, xpeer).wait_recv()
+        branch = jnp.dot(attx[d], w_all, preferred_element_type=F32)
         if d:
             send[d] = branch.astype(BF16)
             out_copy(d, ki).start()
@@ -375,25 +384,30 @@
         p2(d, tp).wait_send()
 
     for z in range(zn):
-        for c in range(NCH):
-            t = z * 2 + xi
-
-            @pl.when(jnp.logical_and(z <= zi, zi < zn - 1))
-            def _():
-                up(t, c).wait_send()
-
-            @pl.when(jnp.logical_and(z >= zi, zi > 0))
-            def _():
-                down(t, c).wait_send()
-
-            across(t, c).wait_send()
+
+        def sent(way):
+            whole = raw.at[z * 2 + xi]
+            remote(whole, whole, rsend.at[way, z], rrecv.at[0, 0], sp, xpeer).wait_send()
+
+        @pl.when(jnp.logical_and(z <= zi, zi < zn - 1))
+        def _():
+            sent(0)
+
+        @pl.when(jnp.logical_and(z >= zi, zi > 0))
+        def _():
+            sent(1)
+
+        sent(2)
     for which in range(3):
         for d in range(1, yn):
             kv_direct(which, d, sp).wait_send()
         for y in range(yn):
             kv_forward(which, y * 2 + ci).wait_send()
-    for c in [wo_z, wo_x, wo_xz] + wo_core + at[1:]:
+    for c in [wo_z, wo_x, wo_xz] + wo_core:
         c.wait_send()
+    for d in range(nq):
+        for r in range(1, 4):
+            at_copy(d, r, xpeer).wait_send()
     for d in range(1, nq):
         out_copy(d, ki).wait_send()
 
@@ -406,7 +420,7 @@
     block_rows = latrows + ctx
     modcols = modw.shape[1]
     zn = ntp // 2
-    qb = latrows // 2
+    qb = 4 * padded
     while qb % 32 == 0 and qb * nsp * block_rows * 4 > 1_000_000:
         qb //= 2
     table = jnp.asarray(rotary_tables(nsp, ntp, rows, padded))
@@ -426,18 +440,19 @@
             pltpu.VMEM((width, 384), BF16),
             pltpu.VMEM((4,) + wout.shape, BF16),
             pltpu.VMEM((2, latrows // 2, 256), F32),
-            pltpu.VMEM((nsp, 8, modcols), F32),
-            pltpu.VMEM((ntp, 8, modcols), F32),
+            pltpu.VMEM((nsp, 2, modcols), F32),
+            pltpu.VMEM((ntp, 2, modcols), F32),
             pltpu.VMEM((ntp, padded, width), BF16),
             pltpu.VMEM((ctx, width), BF16),
             pltpu.VMEM((nsp, block_rows, 256), BF16),
             pltpu.VMEM((2, latrows, 128), BF16),
             pltpu.VMEM((latrows, 128), BF16),
-            pltpu.VMEM((latrows // 4, 512), BF16),
+            pltpu.VMEM((zn // 2, padded, 512), BF16),
             pltpu.VMEM((zn // 2, padded, width), BF16),
             pltpu.VMEM((zn // 2, padded, width), BF16),
-            dma((11,)), dma((3, ntp, NCH)), dma((ntp, NCH)), dma((nsp,)), dma((nsp,)), dma((ntp,)),
-            dma((ntp,)), dma((3, nsp)), dma((3, nsp)), dma((3, nsp)), dma((6,)), dma((4, 2)), dma((4,)), dma((4,)),
+            dma((11,)), dma((3, ntp // 2)), dma((ntp, NCH)), dma((nsp,)), dma((nsp,)), dma((ntp,)),
+            dma((ntp,)), dma((3, nsp)), dma((3, nsp)), dma((3, nsp)), dma((6,)), dma((4, 2)), dma((zn // 2, 4)),
+            dma((zn // 2, 4)),
             dma((zn // 2,)), dma((zn // 2,)),
         ],
         compiler_params=pltpu.CompilerParams(

time: 49.9 us -> 46 us (0.922)
  Pallas kernels: 47.4 us -> 43.6 us
    pallas_call x1, Pallas kernels: 47.4 us -> 43.6 us  [shards(): pl.pallas_call(functools.partial(kernel, nsp, ntp, rows, padded, ctx, wid...]
where the time goes in v4:
time: 46 us; the launch traced here: 45.8 us
  Pallas kernels  43.6 us (95%)
  local copies, waits for them, and re-layouts  1.57 us (3%)
  between operations  0.66 us (1%)
    pallas_call x1, Pallas kernels, shards(): pl.pallas_call(functools.partial(kernel, nsp, ntp, rows, padded, ctx, wid...  43.6 us
    unnamed x1, local copies, waits for them, and re-layouts  1.57 us

profile of v4, /device:TPU:0, one launch (start us, length us, event | category | flops | bytes accessed | tf_op | source)
XLA Modules:
  0.0 45.8 jit_solution(2922056838273616378)
XLA Ops:
  0.7 43.6 %shard_map.109 = bf16[30,2048]{1,0:T(8,128)(2,1)} custom-call(bf16[30,2048]{1,0:T(8,128)(2,1)} %latent.1, bf16[192,2048]{1,0:T(8,128)(2,1)} %context.1, f32[512]{0:T(512)} %condl.1, f32[512]{0:T(512)} %condc.1, bf16[512,768]{1,0:T(8,128)(2,1)} %modw.1, bf16[2048,128]{1,0:T(8,128)(2,1)} %wq.1, bf16[2048,128]{1,0:T(8,128)(2,1)} %wk.1, bf16[2048,128]{1,0:T(8,128)(2,1)} %wv.1, ...), custom_call_target="tpu_custom_call" | custom-call | tf_op jit(solution)/shard_map/pallas_call | solution.py:431
  44.2 1.6 %copy.14 = bf16[30,2048]{1,0:T(8,128)(2,1)} copy(bf16[30,2048]{1,0:T(8,128)(2,1)} %shard_map.109) | data formatting | bytes 245760

commit v5 on v4

--- a/solution.py
+++ b/solution.py
@@ -292,9 +292,6 @@
     for i in range(8, 11):
         copies[i].wait()
     project(0)
-    wo_z.wait_recv()
-    wo_xz.start()
-    wo_core[0].start()
     kv_relay(2)
     for i in range(zn):
         t = position(i) * 2 + (1 - xi)
@@ -303,6 +300,9 @@
         nbuf[zn + i, 0:rows, :] = normed(raw[t], scale_l, shift_l)
     kv_relay(0)
     project(1)
+    wo_z.wait_recv()
+    wo_xz.start()
+    wo_core[0].start()
     kv_relay(1)
     kv_finish(2)
     kv_finish(0)
@@ -346,11 +346,10 @@
         for r, to in ((3, xzpeer), (2, xpeer), (1, zpeer)):
             at_copy(d, r, to).start()
 
-    attended(nq - 1)
+    for d in range(nq - 1, -1, -1):
+        attended(d)
     wo_x.wait_recv()
     wo_core[1].start()
-    for d in range(nq - 2, -1, -1):
-        attended(d)
     wo_xz.wait_recv()
     wo_core[2].start()
     for r in range(1, 4):

time: 46 us -> 45.3 us (0.985)
  Pallas kernels: 43.6 us -> 42.9 us
    pallas_call x1, Pallas kernels: 43.6 us -> 42.9 us  [shards(): pl.pallas_call(functools.partial(kernel, nsp, ntp, rows, padded, ctx, wid...]
where the time goes in v5:
time: 45.3 us; the launch traced here: 45.1 us
  Pallas kernels  42.9 us (95%)
  local copies, waits for them, and re-layouts  1.57 us (3%)
  between operations  0.66 us (1%)
    pallas_call x1, Pallas kernels, shards(): pl.pallas_call(functools.partial(kernel, nsp, ntp, rows, padded, ctx, wid...  42.9 us
    unnamed x1, local copies, waits for them, and re-layouts  1.57 us

profile of v5, /device:TPU:0, one launch (start us, length us, event | category | flops | bytes accessed | tf_op | source)
XLA Modules:
  0.0 45.1 jit_solution(18282885938088015121)
XLA Ops:
  0.7 42.9 %shard_map.109 = bf16[30,2048]{1,0:T(8,128)(2,1)} custom-call(bf16[30,2048]{1,0:T(8,128)(2,1)} %latent.1, bf16[192,2048]{1,0:T(8,128)(2,1)} %context.1, f32[512]{0:T(512)} %condl.1, f32[512]{0:T(512)} %condc.1, bf16[512,768]{1,0:T(8,128)(2,1)} %modw.1, bf16[2048,128]{1,0:T(8,128)(2,1)} %wq.1, bf16[2048,128]{1,0:T(8,128)(2,1)} %wk.1, bf16[2048,128]{1,0:T(8,128)(2,1)} %wv.1, ...), custom_call_target="tpu_custom_call" | custom-call | tf_op jit(solution)/shard_map/pallas_call | solution.py:430
  43.6 1.6 %copy.14 = bf16[30,2048]{1,0:T(8,128)(2,1)} copy(bf16[30,2048]{1,0:T(8,128)(2,1)} %shard_map.109) | data formatting | bytes 245760
